TPU v7x, 32 devices: a whole 2x2x4 slice. The times are simulated.
32 devices in a mesh: ep: 8 (over z, y), tp: 4 (over x, core).
Axes of the slice: x: 2, y: 2, z: 4, core: 2. Of those that a mesh axis runs over, the one named last changes fastest.
Arguments:
- mixer_input: bfloat16 [4096, 2048], P('ep'), may hold values from -6 to 6
- log_forget_total: float32 [16, 4096], P('tp'), may hold values from -684 to 0, as said below
- mixer_gain: float32 [2048], replicated, may hold values from 0.1 to 1.9
- w_query: bfloat16 [2048, 1024], P(None, 'tp'), may hold values from -1 to 1
- w_key: bfloat16 [2048, 256], P(None, 'tp'), may hold values from -8 to 8
- w_value: bfloat16 [2048, 256], P(None, 'tp'), may hold values from -0.125 to 0.125
- w_output: bfloat16 [1024, 2048], replicated, may hold values from -0.1875 to 0.1875
- mixer_post_gain: float32 [2048], replicated, may hold values from 0.1 to 1.9
- expert_input: bfloat16 [2048, 2048], P('ep'), may hold values from -6 to 6
- expert_ids: int32 [2048, 2], P('ep'), may hold values from 0 to 7, all different within a row; in each aligned block of 64 rows (0 to 63, 64 to 127, ...) at most 32 rows name the same one
- route_weight: float32 [2048, 2], P('ep'), may hold values from 0.1 to 1
- expert_gain: float32 [2048], replicated, may hold values from 0.1 to 1.9
- w_gate: bfloat16 [8, 2048, 3584], P('ep', None, 'tp'), may hold values from -0.125 to 0.125
- w_up: bfloat16 [8, 2048, 3584], P('ep', None, 'tp'), may hold values from -0.125 to 0.125
- w_down: bfloat16 [8, 3584, 2048], P('ep', 'tp'), may hold values from -0.09375 to 0.09375
- expert_post_gain: float32 [2048], replicated, may hold values from 0.1 to 1.9
Outputs:
- mixer_out: bfloat16 [4096, 2048], P(('ep', 'tp'))
- expert_out: bfloat16 [2048, 2048], P(('ep', 'tp'))
Inputs may be any that keep to these rules, and one draw needn't show every extreme that they name: `expert_ids`: in each aligned block of 64 tokens no expert is named by more than 32 of them. `log_forget_total`: each head's values never rise along the positions.
All inputs are finite; a program needn't handle non-finite values.
Results may differ from a plain program's by a relative error of at most 0.012.
The roundings to bfloat16 on the way count: a program that leaves them out, or rounds other values in their place, can miss the bound.
Values may be sent and summed in bfloat16 or wider, within the bound.
A program may use at most 128 MiB of HBM per device.

v0:
```python
import math
import jax
import jax.numpy as jnp
from jax import lax
from jax.sharding import PartitionSpec as P

HD = 64
TOP_K = 2
NEG_FILL = -1e30
NORM_EPS = 1e-06


def norm_rows(values_in, gain_vec):
    widened = values_in.astype(jnp.float32)
    return (
        widened
        * lax.rsqrt(jnp.mean(widened * widened, axis=-1, keepdims=True) + NORM_EPS)
        * gain_vec
    )


def unchanged(present_state):
    return present_state


def mixer_half(
    mixer_input, log_forget_total, mixer_gain, w_query, w_key, w_value, w_output, mixer_post_gain
):
    row_count = mixer_input.shape[0]
    offset = lax.axis_index("ep") * row_count
    head_local = w_query.shape[1] // HD
    kv_local = w_key.shape[1] // HD
    group_size = head_local // kv_local
    normed = norm_rows(mixer_input, mixer_gain).astype(jnp.bfloat16)
    queries = (
        jnp.dot(normed, w_query, preferred_element_type=jnp.float32)
        .astype(jnp.bfloat16)
        .reshape(row_count, kv_local, group_size, HD)
    )
    key_rows = (
        jnp.dot(normed, w_key, preferred_element_type=jnp.float32)
        .astype(jnp.bfloat16)
        .reshape(row_count, kv_local, HD)
    )
    value_rows = (
        jnp.dot(normed, w_value, preferred_element_type=jnp.float32)
        .astype(jnp.bfloat16)
        .reshape(row_count, kv_local, HD)
    )
    gate_totals = log_forget_total.reshape(kv_local, group_size, -1)
    query_gate = lax.dynamic_slice_in_dim(gate_totals, offset, row_count, 2)
    query_pos = offset + jnp.arange(row_count, dtype=jnp.int32)
    last_row = offset + row_count - 1
    score_scale = HD ** (-0.5)
    start_state = (
        jnp.full((kv_local, group_size, row_count), NEG_FILL, jnp.float32),
        jnp.zeros((kv_local, group_size, row_count), jnp.float32),
        jnp.zeros((kv_local, group_size, row_count, HD), jnp.float32),
    )
    running = start_state
    key_piece = lax.all_gather(key_rows, "ep", axis=0, tiled=True)
    value_piece = lax.all_gather(value_rows, "ep", axis=0, tiled=True)
    piece_rows = key_piece.shape[0]
    block_rows = math.gcd(piece_rows, 512)
    block_total = piece_rows // block_rows
    key_blocks = key_piece.reshape(block_total, block_rows, kv_local, HD)
    value_blocks = value_piece.reshape(block_total, block_rows, kv_local, HD)

    def one_block(present_state, operands):
        key_block, value_block, block_index = operands
        block_first = block_index * block_rows

        def update(prior_value):
            row_max, denominator, numerator = prior_value
            key_gate = lax.dynamic_slice_in_dim(gate_totals, block_first, block_rows, 2)
            scores = (
                jnp.einsum("qgjd,kgd->gjqk", queries, key_block, preferred_element_type=jnp.float32)
                * score_scale
            )
            scores = scores + query_gate[:, :, :, None] - key_gate[:, :, None, :]
            visible = (block_first + jnp.arange(block_rows, dtype=jnp.int32))[None, :] <= query_pos[
                :, None
            ]
            scores = jnp.where(visible, scores, NEG_FILL)
            new_max = jnp.maximum(row_max, jnp.max(scores, axis=-1))
            shifted = jnp.where(visible, jnp.exp(scores - new_max[..., None]), 0.0)
            factor = jnp.exp(row_max - new_max)
            denominator = denominator * factor + jnp.sum(shifted, axis=-1)
            numerator = numerator * factor[..., None] + jnp.einsum(
                "gjqk,kgd->gjqd",
                shifted.astype(jnp.bfloat16),
                value_block,
                preferred_element_type=jnp.float32,
            )
            return (new_max, denominator, numerator)

        return (lax.cond(block_first <= last_row, update, unchanged, present_state), None)

    running, _ = lax.scan(
        one_block, running, (key_blocks, value_blocks, jnp.arange(block_total, dtype=jnp.int32))
    )
    row_max, denominator, numerator = running
    mixed_heads = (
        jnp.transpose(numerator / denominator[..., None], (2, 0, 1, 3))
        .reshape(row_count, head_local * HD)
        .astype(jnp.bfloat16)
    )
    by_rows = lax.all_to_all(mixed_heads, "tp", split_axis=0, concat_axis=1, tiled=True)
    projected = jnp.dot(by_rows, w_output, preferred_element_type=jnp.float32)
    return norm_rows(projected, mixer_post_gain).astype(jnp.bfloat16)


def expert_half(
    expert_input, expert_ids, route_weight, expert_gain, w_gate, w_up, w_down, expert_post_gain
):
    row_count = expert_input.shape[0]
    quarters = lax.axis_size("tp")
    experts = lax.axis_size("ep")
    quarter_rows = row_count // quarters
    slot_count = 2 * TOP_K * quarter_rows // experts
    own_quarter = lax.axis_index("tp")
    normed = norm_rows(expert_input, expert_gain).astype(jnp.bfloat16)
    padded_rows = jnp.concatenate([normed, jnp.zeros((1, normed.shape[1]), jnp.bfloat16)], axis=0)
    routed = expert_ids.reshape(quarters, quarter_rows * TOP_K)
    matches = (routed[:, :, None] == jnp.arange(experts, dtype=jnp.int32)[None, None, :]).astype(
        jnp.int32
    )
    slot_ranks = jnp.sum(jnp.cumsum(matches, axis=1) * matches, axis=2) - 1
    owners = (jnp.arange(row_count * TOP_K, dtype=jnp.int32) // TOP_K).reshape(
        quarters, quarter_rows * TOP_K
    )
    quarter_index = jnp.broadcast_to(jnp.arange(quarters, dtype=jnp.int32)[:, None], routed.shape)
    slot_table = (
        jnp.full((quarters, slot_count, experts), row_count, jnp.int32)
        .at[quarter_index, slot_ranks, routed]
        .set(owners)
    )
    gate_local = w_gate[0]
    up_local = w_up[0]
    down_local = w_down[0]
    unit_count = gate_local.shape[1]
    own_table = lax.dynamic_index_in_dim(slot_table, own_quarter, 0, keepdims=False)
    outgoing = padded_rows[own_table]
    arrived = lax.all_to_all(outgoing, "ep", split_axis=1, concat_axis=1, tiled=True)
    slot_rows = lax.all_gather(arrived[None], "tp", axis=0, tiled=True)
    flat_rows = slot_rows.reshape(-1, slot_rows.shape[-1])
    gate_part = jnp.dot(flat_rows, gate_local, preferred_element_type=jnp.float32)
    up_part = jnp.dot(flat_rows, up_local, preferred_element_type=jnp.float32)
    hidden = (
        (jax.nn.silu(gate_part) * up_part)
        .astype(jnp.bfloat16)
        .reshape(slot_rows.shape[:-1] + (unit_count,))
    )
    product = jnp.dot(
        hidden.reshape(-1, unit_count), down_local, preferred_element_type=jnp.float32
    )
    summed = lax.psum_scatter(
        product.reshape(lax.axis_size("tp") * 1, slot_count, experts, product.shape[-1]).astype(
            jnp.bfloat16
        ),
        "tp",
        scatter_dimension=0,
        tiled=True,
    ).astype(jnp.float32)
    results = summed[0].astype(jnp.bfloat16)
    returned = lax.all_to_all(results, "ep", split_axis=1, concat_axis=1, tiled=True)
    flat_results = returned.reshape(slot_count * experts, returned.shape[-1])
    own_routes = lax.dynamic_index_in_dim(routed, own_quarter, 0, keepdims=False)
    own_ranks = lax.dynamic_index_in_dim(slot_ranks, own_quarter, 0, keepdims=False)
    picked = flat_results[own_ranks * experts + own_routes].reshape(quarter_rows, TOP_K, -1)
    own_weights = lax.dynamic_slice_in_dim(
        route_weight, own_quarter * quarter_rows, quarter_rows, 0
    )
    combined = jnp.sum(own_weights[:, :, None] * picked.astype(jnp.float32), axis=1)
    return norm_rows(combined, expert_post_gain).astype(jnp.bfloat16)


def per_device(
    mixer_input,
    log_forget_total,
    mixer_gain,
    w_query,
    w_key,
    w_value,
    w_output,
    mixer_post_gain,
    expert_input,
    expert_ids,
    route_weight,
    expert_gain,
    w_gate,
    w_up,
    w_down,
    expert_post_gain,
):
    mixer_out = mixer_half(
        mixer_input,
        log_forget_total,
        mixer_gain,
        w_query,
        w_key,
        w_value,
        w_output,
        mixer_post_gain,
    )
    expert_out = expert_half(
        expert_input, expert_ids, route_weight, expert_gain, w_gate, w_up, w_down, expert_post_gain
    )
    return (mixer_out, expert_out)


def solution(mesh):
    placed = (
        P("ep", None),
        P("tp", None),
        P(),
        P(None, "tp"),
        P(None, "tp"),
        P(None, "tp"),
        P(),
        P(),
        P("ep", None),
        P("ep", None),
        P("ep", None),
        P(),
        P("ep", None, "tp"),
        P("ep", None, "tp"),
        P("ep", "tp", None),
        P(),
    )
    return jax.shard_map(
        per_device,
        mesh=mesh,
        in_specs=placed,
        out_specs=(P(("ep", "tp"), None), P(("ep", "tp"), None)),
        check_vma=False,
    )
```

profile of v0, /device:TPU:0, one launch (start us, length us, event | category | flops | bytes accessed | tf_op | source)
XLA Modules:
  0.0 324.2 jit_solution(3863174267052389493)
XLA Ops:
  7.2 0.9 copy.41
  9.2 29.5 %scatter_fusion = s32[4,32,8]{1,2,0:T(8,128)S(1)} fusion(s32[4,32,8]{1,2,0:T(8,128)S(1)} %broadcast_in_dim.39, s32[512]{0:T(512)S(1)} %fusion.52, s32[512]{0:T(512)S(1)} %fusion.54), kind=kCustom, calls=%fused_computation.2 | custom fusion | bytes 12288 | tf_op jit(solution)/shard_map/scatter | solution.py:136
  39.7 1.4 gather_fusion
  41.0 0.6 copy.44
  41.6 32.9 %all_to_all.26 = bf16[32,8,2048]{2,0,1:T(8,128)(2,1)S(1)} all-to-all(bf16[32,8,2048]{2,0,1:T(8,128)(2,1)S(1)} %copy.44), channel_id=1, replica_groups=mesh['ep'=8,'tp'=4] {'ep'}, dimensions={1} | all-to-all | bytes 2097152 | tf_op jit(solution)/shard_map/all_to_all | solution.py:144
  74.5 1.6 copy.45
  76.3 33.4 %all-gather.5.cloned.1.call-done = bf16[128,8,2048]{2,1,0:T(8,128)(2,1)} async-done(((bf16[32,8,2048]{2,1,0:T(8,128)(2,1)}), bf16[128,8,2048]{2,1,0:T(8,128)(2,1)}) %all-gather.5.cloned.1.call-update) | async-done | bytes 4194320 | tf_op jit(solution)/shard_map/all_gather | solution.py:145
  109.7 7.5 %fusion.32 = f32[1024,896]{1,0:T(8,128)S(1)} fusion(bf16[128,8,2048]{2,1,0:T(8,128)(2,1)} %all-gather.5.cloned.1.call-done, bf16[1,2048,896]{2,1,0:T(8,128)(2,1)} %param.33), kind=kOutput, calls=%fused_computation.40 | convolution fusion | flops 3758096384 | bytes 11534336 | tf_op jit(solution)/shard_map/dot_general | solution.py:148
  117.2 4.8 %multiply_convert_fusion = bf16[1024,896]{1,0:T(8,128)(2,1)S(1)} fusion(f32[1024,896]{1,0:T(8,128)S(1)} %fusion.32, bf16[1,2048,896]{2,1,0:T(8,128)(2,1)S(1)} %copy-done.11, bf16[128,8,2048]{2,1,0:T(8,128)(2,1)S(1)} %copy-done.10), kind=kOutput, calls=%fused_computation.48 | convolution fusion | flops 3763601408 | bytes 13369344 | tf_op jit(solution)/shard_map/dot_general | solution.py:147
  122.0 6.0 %convolution_convert_fusion = bf16[4,32,8,2048]{3,2,1,0:T(8,128)(2,1)} fusion(bf16[4,32,8,896]{3,2,1,0:T(8,128)(2,1)S(1)} %bitcast.163, bf16[1,896,2048]{2,1,0:T(8,128)(2,1)S(1)} %copy-done.12), kind=kOutput, calls=%fused_computation.44 | convolution fusion | flops 3760193536 | bytes 9699328 | tf_op jit(solution)/shard_map/dot_general | solution.py:154
  128.0 1.5 copy-done.1
  129.6 0.5 fusion.29
  130.1 2.2 fusion.31
  132.3 0.8 convolution_convert_fusion.3
  133.0 31.5 %all-gather = bf16[4096,64]{0,1:T(8,128)(2,1)S(1)} all-gather(bf16[512,64]{0,1:T(8,128)(2,1)S(1)} %convolution_convert_fusion.3), channel_id=2, replica_groups=mesh['ep'=8,'tp'=4] {'ep'}, dimensions={0}, use_global_device_ids=true | all-gather | bytes 589824 | tf_op jit(solution)/shard_map/all_gather | solution.py:61
  164.7 0.9 copy.37
  165.6 0.8 convolution_convert_fusion.2
  166.4 31.4 %all-gather.1 = bf16[4096,64]{0,1:T(8,128)(2,1)S(1)} all-gather(bf16[512,64]{0,1:T(8,128)(2,1)S(1)} %convolution_convert_fusion.2), channel_id=3, replica_groups=mesh['ep'=8,'tp'=4] {'ep'}, dimensions={0}, use_global_device_ids=true | all-gather | bytes 589824 | tf_op jit(solution)/shard_map/all_gather | solution.py:62
  198.0 1.0 copy.38
  199.0 0.7 dynamic-slice_bitcast_fusion.1
  199.7 1.5 convolution_convert_fusion.1
  201.2 18.1 %while.15 = (s32[]{:T(128)}, f32[1,4,512]{2,1,0:T(4,128)S(1)}, f32[1,4,512]{2,1,0:T(4,128)S(1)}, f32[1,4,512,64]{2,3,1,0:T(8,128)S(1)}, s32[8]{0:T(128)S(1)}, /*...) while((s32[]{:T(128)}, f32[1,4,512]{2,1,0:T(4,128)S(1)}, ...), condition=%wide.region_6.7_spmd.clone, body=%wide.region_1.6_spmd.clone.sunk | while | flops 288889856 | bytes 15283569 | solution.py:99
  201.2 0.7 dynamic_slice.79
  202.5 7.4 %conditional.3 = ((f32[1,4,512]{2,1,0:T(4,128)S(1)}, f32[1,4,512]{2,1,0:T(4,128)S(1)}, f32[1,4,512,64]{2,3,1,0:T(8,128)S(1)})) conditional(s32[]{:T(128)} %convert_element_type.123, (f32[1,4,512]{2,1,0:T(4,128)S(1)}, f32[1,4,512]{2,1,0:T(4,128)S(1)}, f32[1,4,512,64]{2,3,1,0:T(8,128)S(1)}) %tuple.48, (s32[]{:T(128)}, s32[]{:T(128)}, ...), branch_computations={%region_2.2_spmd, %region_3.5_spmd} | conditional | flops 288889856 | bytes 15281230 | solution.py:97
  202.5 0.8 dynamic-slice_bitcast_fusion
  203.6 2.2 fusion.6
  205.8 2.6 fusion.14
  208.4 1.5 fusion.5
  210.0 0.7 dynamic_slice.79
  211.3 0.7 dynamic_slice.79
  212.6 0.7 dynamic_slice.79
  214.0 0.7 dynamic_slice.79
  215.3 0.7 dynamic_slice.79
  216.7 0.7 dynamic_slice.79
  218.0 0.7 dynamic_slice.79
  219.5 0.7 copy.39
  220.2 3.4 %all-to-all-start = ((bf16[4,128,256]{1,2,0:T(8,128)(2,1)}), bf16[4,128,256]{1,2,0:T(8,128)(2,1)S(1)}, u32[]{:S(2)}, u32[]{:S(2)}) async-start(bf16[4,128,256]{1,2,0:T(8,128)(2,1)} %copy.39), calls=%async_computation | async-start | bytes 524288 | tf_op jit(solution)/shard_map/all_to_all | solution.py:108
  223.7 2.8 copy.46
  226.5 3.1 all-to-all-done
  229.6 57.5 %all-to-all-start.2 = ((bf16[32,8,2048]{2,0,1:T(8,128)(2,1)}), bf16[32,8,2048]{2,0,1:T(8,128)(2,1)S(1)}, u32[]{:S(2)}, u32[]{:S(2)}) async-start(bf16[32,8,2048]{2,0,1:T(8,128)(2,1)} %copy.46), calls=%async_computation.3 | async-start | bytes 2097152 | tf_op jit(solution)/shard_map/all_to_all | solution.py:166
  287.3 3.0 multiply_reduce_fusion.1
  290.3 1.0 multiply_convert_fusion.1
  291.3 21.4 %all-to-all-done.2 = bf16[32,8,2048]{2,0,1:T(8,128)(2,1)S(1)} async-done(((bf16[32,8,2048]{2,0,1:T(8,128)(2,1)}), bf16[32,8,2048]{2,0,1:T(8,128)(2,1)S(1)}, u32[]{:S(2)}, u32[]{:S(2)}) %all-to-all-start.2) | async-done | bytes 1048608 | tf_op jit(solution)/shard_map/all_to_all | solution.py:166
  312.7 0.6 copy.53
  313.3 0.9 gather_fusion.1
  314.2 0.7 reshape.287
  314.9 1.5 multiply_reduce_fusion
  316.6 0.8 multiply_convert_fusion.2
  (83 shorter events, 3.4 us)
Async XLA Ops:
  7.2 192.5 %copy-start = (bf16[2048,256]{1,0:T(8,128)(2,1)S(1)}, bf16[2048,256]{1,0:T(8,128)(2,1)}, u32[]{:S(2)}) copy-start(bf16[2048,256]{1,0:T(8,128)(2,1)} %param.23) | copy-start | bytes 3145732
  7.2 31.8 %copy-start.2 = (bf16[256,2048]{1,0:T(8,128)(2,1)S(1)}, bf16[256,2048]{1,0:T(8,128)(2,1)}, u32[]{:S(2)}) copy-start(bf16[256,2048]{1,0:T(8,128)(2,1)} %param.28) | copy-start | bytes 3145732
  7.2 32.1 %copy-start.5 = (f32[2048]{0:T(1024)S(1)}, f32[2048]{0:T(1024)}, u32[]{:S(2)}) copy-start(f32[2048]{0:T(1024)} %param.31) | copy-start | bytes 24580
  7.2 102.5 %all-gather.5.cloned.1.call-start = ((), (), s32[]{:S(2)}) async-start(), calls=%async_computation.5 | async-start | bytes 5242880 | tf_op jit(solution)/shard_map/all_gather | solution.py:145
  76.1 147.6 %reduce-scatter.2.cloned.1.call-start = ((), (), s32[]{:S(2)}) async-start(), calls=%async_computation.4 | async-start | bytes 5242880 | tf_op jit(solution)/shard_map/reduce_scatter | solution.py:157
  109.7 7.5 %copy-start.10 = (bf16[128,8,2048]{2,1,0:T(8,128)(2,1)S(1)}, bf16[128,8,2048]{2,1,0:T(8,128)(2,1)}, u32[]{:S(2)}) copy-start(bf16[128,8,2048]{2,1,0:T(8,128)(2,1)} %all-gather.5.cloned.1.call-done) | copy-start | bytes 12582916
  109.7 7.5 %copy-start.11 = (bf16[1,2048,896]{2,1,0:T(8,128)(2,1)S(1)}, bf16[1,2048,896]{2,1,0:T(8,128)(2,1)}, u32[]{:S(2)}) copy-start(bf16[1,2048,896]{2,1,0:T(8,128)(2,1)} %param.32) | copy-start | bytes 11010052
  117.2 4.8 %copy-start.12 = (bf16[1,896,2048]{2,1,0:T(8,128)(2,1)S(1)}, bf16[1,896,2048]{2,1,0:T(8,128)(2,1)}, u32[]{:S(2)}) copy-start(bf16[1,896,2048]{2,1,0:T(8,128)(2,1)} %param.34) | copy-start | bytes 11010052
  128.0 1.6 copy-start.1
  128.0 2.1 copy-start.6
  128.0 4.3 %copy-start.3 = (bf16[2048,64]{0,1:T(8,128)(2,1)S(1)}, bf16[2048,64]{0,1:T(8,128)(2,1)}, u32[]{:S(2)}) copy-start(bf16[2048,64]{0,1:T(8,128)(2,1)} %param.24) | copy-start | bytes 786436
  130.1 35.5 %copy-start.4 = (bf16[2048,64]{0,1:T(8,128)(2,1)S(1)}, bf16[2048,64]{0,1:T(8,128)(2,1)}, u32[]{:S(2)}) copy-start(bf16[2048,64]{0,1:T(8,128)(2,1)} %param.25) | copy-start | bytes 786436
  219.4 67.7 %copy-start.9 = (f32[256,2]{0,1:T(2,128)S(1)}, f32[256,2]{0,1:T(2,128)}, u32[]{:S(2)}) copy-start(f32[256,2]{0,1:T(2,128)} %param.30) | copy-start | bytes 6148
  220.2 9.4 %all-to-all-start = ((bf16[4,128,256]{1,2,0:T(8,128)(2,1)}), bf16[4,128,256]{1,2,0:T(8,128)(2,1)S(1)}, u32[]{:S(2)}, u32[]{:S(2)}) async-start(bf16[4,128,256]{1,2,0:T(8,128)(2,1)} %copy.39), calls=%async_computation | async-start | bytes 524288 | tf_op jit(solution)/shard_map/all_to_all | solution.py:108
  226.5 63.9 %copy-start.7 = (f32[2048]{0:T(1024)S(1)}, f32[2048]{0:T(1024)}, u32[]{:S(2)}) copy-start(f32[2048]{0:T(1024)} %param.27) | copy-start | bytes 24580
  229.6 83.1 %all-to-all-start.2 = ((bf16[32,8,2048]{2,0,1:T(8,128)(2,1)}), bf16[32,8,2048]{2,0,1:T(8,128)(2,1)S(1)}, u32[]{:S(2)}, u32[]{:S(2)}) async-start(bf16[32,8,2048]{2,0,1:T(8,128)(2,1)} %copy.46), calls=%async_computation.3 | async-start | bytes 2097152 | tf_op jit(solution)/shard_map/all_to_all | solution.py:166
  313.3 3.3 %copy-start.8 = (f32[2048]{0:T(1024)S(1)}, f32[2048]{0:T(1024)}, u32[]{:S(2)}) copy-start(f32[2048]{0:T(1024)} %param.35) | copy-start | bytes 24580
Sparse Core Ops, SparseCore 0:
  76.2 33.4 all-gather.4
  128.1 44.5 reduce-scatter.1
where the time goes:
time: 326 us; the launch traced here: 324 us
  blocking collectives  95.8 us (29%)
  starting transfers between devices  61.1 us (19%)
  waiting for transfers between devices  58 us (18%)
  local copies, waits for them, and re-layouts  51.1 us (16%)
  matrix products  29 us (9%)
  between operations  14.4 us (4%)
  other arithmetic  9.24 us (3%)
  loops' own time  5.57 us (2%)
    all_to_all x1, starting transfers between devices, expert_half(): lax.all_to_all(results, 'ep', split_axis=1, concat_axis=1, tiled=True)  57.5 us
    all_gather x1, waiting for transfers between devices, expert_half(): slot_rows = lax.all_gather(arrived[None], 'tp', axis=0, tiled=True)  33.4 us
    all_to_all x1, blocking collectives, expert_half(): lax.all_to_all(outgoing, 'ep', split_axis=1, concat_axis=1, tiled=True)  32.9 us
    all_gather x1, blocking collectives, mixer_half(): key_piece = lax.all_gather(key_rows, 'ep', axis=0, tiled=True)  31.5 us
    all_gather x1, blocking collectives, mixer_half(): value_piece = lax.all_gather(value_rows, 'ep', axis=0, tiled=True)  31.4 us
    scatter x1, local copies, waits for them, and re-layouts, expert_half(): slot_table = jnp.full((quarters, slot_count, experts), row_count, jnp.int...  29.5 us
    all_to_all x1, waiting for transfers between devices, expert_half(): lax.all_to_all(results, 'ep', split_axis=1, concat_axis=1, tiled=True)  21.4 us
    dot_general x1, matrix products, expert_half(): up_part = jnp.dot(flat_rows, up_local, preferred_element_type=jnp.float32)  7.49 us
  transfers between devices with their start and end apart: 4, of which 3 were waited for; matrix products, arithmetic and copies ran while one was open for 9% of the time, Pallas kernels for 0%

commit v1 on v0

--- a/solution.py
+++ b/solution.py
@@ -58,7 +58,24 @@
         jnp.zeros((kv_local, group_size, row_count, HD), jnp.float32),
     )
     running = start_state
-    key_piece = lax.all_gather(key_rows, "ep", axis=0, tiled=True)
+
+    def _point_stops_all(shard_in, axis_name):
+        q_n = lax.axis_size(axis_name)
+        block_list = [shard_in]
+        for hop_no in range(q_n - 1):
+            block_list.append(
+                lax.ppermute(
+                    block_list[-1], axis_name, [(src_i, (src_i + 1) % q_n) for src_i in range(q_n)]
+                )
+            )
+        passed = jnp.roll(
+            jnp.concatenate(block_list[::-1], axis=0),
+            (lax.axis_index(axis_name) + 1) * shard_in.shape[0],
+            0,
+        )
+        return passed
+
+    key_piece = _point_stops_all(key_rows, axis_name="ep")
     value_piece = lax.all_gather(value_rows, "ep", axis=0, tiled=True)
     piece_rows = key_piece.shape[0]
     block_rows = math.gcd(piece_rows, 512)

time: 326 us -> 313 us (0.960)
  waiting for transfers between devices: 58 us -> 94.5 us
  blocking collectives: 95.8 us -> 64.5 us
  starting transfers between devices: 61.1 us -> 49.3 us
    ppermute x0 -> x7, waiting for transfers between devices: none -> 36.5 us  [_point_stops_all(): lax.ppermute(block_list[-1], axis_name, [(src_i, (src_i + 1) % q_n) for s...]
    all_gather x1 -> x0, blocking collectives: 31.5 us -> none  [mixer_half(): key_piece = lax.all_gather(key_rows, 'ep', axis=0, tiled=True)]
    all_to_all x1, starting transfers between devices: 57.5 us -> 42 us  [expert_half(): lax.all_to_all(results, 'ep', split_axis=1, concat_axis=1, tiled=True)]
    ppermute x0 -> x7, starting transfers between devices: none -> 3.64 us  [_point_stops_all(): lax.ppermute(block_list[-1], axis_name, [(src_i, (src_i + 1) % q_n) for s...]
  transfers between devices with their start and end apart: 4 -> 11, of which waited for: 3 -> 9; matrix products, arithmetic and copies ran while one was open for 9% -> 7% of each run, Pallas kernels for 0% -> 0%
where the time goes in v1:
time: 313 us; the launch traced here: 312 us
  waiting for transfers between devices  94.5 us (30%)
  blocking collectives  64.5 us (21%)
  local copies, waits for them, and re-layouts  49.5 us (16%)
  starting transfers between devices  49.3 us (16%)
  matrix products  26.5 us (8%)
  between operations  14.6 us (5%)
  other arithmetic  7.61 us (2%)
  loops' own time  6.04 us (2%)
    all_to_all x1, starting transfers between devices, expert_half(): lax.all_to_all(results, 'ep', split_axis=1, concat_axis=1, tiled=True)  42 us
    ppermute x7, waiting for transfers between devices, _point_stops_all(): lax.ppermute(block_list[-1], axis_name, [(src_i, (src_i + 1) % q_n) for s...  36.5 us
    all_gather x1, waiting for transfers between devices, expert_half(): slot_rows = lax.all_gather(arrived[None], 'tp', axis=0, tiled=True)  33.4 us
    all_to_all x1, blocking collectives, expert_half(): lax.all_to_all(outgoing, 'ep', split_axis=1, concat_axis=1, tiled=True)  32.9 us
    all_gather x1, blocking collectives, mixer_half(): value_piece = lax.all_gather(value_rows, 'ep', axis=0, tiled=True)  31.6 us
    scatter x1, local copies, waits for them, and re-layouts, expert_half(): slot_table = jnp.full((quarters, slot_count, experts), row_count, jnp.int...  29.5 us
    all_to_all x1, waiting for transfers between devices, expert_half(): lax.all_to_all(results, 'ep', split_axis=1, concat_axis=1, tiled=True)  21.4 us
    dot_general x1, matrix products, expert_half(): up_part = jnp.dot(flat_rows, up_local, preferred_element_type=jnp.float32)  7.49 us
  transfers between devices with their start and end apart: 11, of which 9 were waited for; matrix products, arithmetic and copies ran while one was open for 7% of the time, Pallas kernels for 0%

profile of v1, /device:TPU:0, one launch (start us, length us, event | category | flops | bytes accessed | tf_op | source)
XLA Modules:
  0.0 312.4 jit_solution(12251461355318069971)
XLA Ops:
  7.2 0.9 copy.40
  9.2 29.5 %scatter_fusion = s32[4,32,8]{1,2,0:T(8,128)S(1)} fusion(s32[4,32,8]{1,2,0:T(8,128)S(1)} %broadcast_in_dim.39, s32[512]{0:T(512)S(1)} %fusion.53, s32[512]{0:T(512)S(1)} %fusion.55), kind=kCustom, calls=%fused_computation.2 | custom fusion | bytes 12288 | tf_op jit(solution)/shard_map/scatter | solution.py:153
  39.7 1.4 gather_fusion
  41.6 32.9 %all_to_all.26 = bf16[32,8,2048]{2,0,1:T(8,128)(2,1)S(1)} all-to-all(bf16[32,8,2048]{2,0,1:T(8,128)(2,1)S(1)} %copy.43), channel_id=1, replica_groups=mesh['ep'=8,'tp'=4] {'ep'}, dimensions={1} | all-to-all | bytes 2097152 | tf_op jit(solution)/shard_map/all_to_all | solution.py:161
  74.5 1.6 copy.44
  76.3 33.4 %all-gather.4.cloned.1.call-done = bf16[128,8,2048]{2,1,0:T(8,128)(2,1)} async-done(((bf16[32,8,2048]{2,1,0:T(8,128)(2,1)}), bf16[128,8,2048]{2,1,0:T(8,128)(2,1)}) %all-gather.4.cloned.1.call-update) | async-done | bytes 4194320 | tf_op jit(solution)/shard_map/all_gather | solution.py:162
  109.7 7.5 %fusion.32 = f32[1024,896]{1,0:T(8,128)S(1)} fusion(bf16[128,8,2048]{2,1,0:T(8,128)(2,1)} %all-gather.4.cloned.1.call-done, bf16[1,2048,896]{2,1,0:T(8,128)(2,1)} %param.33), kind=kOutput, calls=%fused_computation.40 | convolution fusion | flops 3758096384 | bytes 11534336 | tf_op jit(solution)/shard_map/dot_general | solution.py:165
  117.2 4.7 %multiply_convert_fusion = bf16[1024,896]{1,0:T(8,128)(2,1)S(1)} fusion(f32[1024,896]{1,0:T(8,128)S(1)} %fusion.32, bf16[1,2048,896]{2,1,0:T(8,128)(2,1)S(1)} %copy-done.11, bf16[128,8,2048]{2,1,0:T(8,128)(2,1)S(1)} %copy-done.10), kind=kOutput, calls=%fused_computation.48 | convolution fusion | flops 3763601408 | bytes 13369344 | tf_op jit(solution)/shard_map/dot_general | solution.py:164
  122.0 6.0 %convolution_convert_fusion = bf16[4,32,8,2048]{3,2,1,0:T(8,128)(2,1)} fusion(bf16[4,32,8,896]{3,2,1,0:T(8,128)(2,1)S(1)} %bitcast.164, bf16[1,896,2048]{2,1,0:T(8,128)(2,1)S(1)} %copy-done.12), kind=kOutput, calls=%fused_computation.44 | convolution fusion | flops 3760193536 | bytes 9699328 | tf_op jit(solution)/shard_map/dot_general | solution.py:171
  128.0 1.6 copy-done.1
  130.7 0.8 fusion.46
  131.4 1.5 collective-permute-start
  132.9 5.5 %collective-permute-done = bf16[512,1,64]{0,2,1:T(8,128)(2,1)S(1)} collective-permute-done((bf16[512,1,64]{0,2,1:T(8,128)(2,1)S(1)}, bf16[512,1,64]{0,2,1:T(8,128)(2,1)S(1)}, u32[]{:S(2)}, u32[]{:S(2)}) %collective-permute-start) | collective-permute-done | bytes 65568 | tf_op jit(solution)/shard_map/ppermute | solution.py:67
  138.4 7.0 %collective-permute-done.1 = bf16[512,1,64]{0,2,1:T(8,128)(2,1)S(1)} collective-permute-done((bf16[512,1,64]{0,2,1:T(8,128)(2,1)S(1)}, bf16[512,1,64]{0,2,1:T(8,128)(2,1)S(1)}, u32[]{:S(2)}, u32[]{:S(2)}) %collective-permute-start.1) | collective-permute-done | bytes 65568 | tf_op jit(solution)/shard_map/ppermute | solution.py:67
  145.4 7.0 %collective-permute-done.2 = bf16[512,1,64]{0,2,1:T(8,128)(2,1)S(1)} collective-permute-done((bf16[512,1,64]{0,2,1:T(8,128)(2,1)S(1)}, bf16[512,1,64]{0,2,1:T(8,128)(2,1)S(1)}, u32[]{:S(2)}, u32[]{:S(2)}) %collective-permute-start.2) | collective-permute-done | bytes 65568 | tf_op jit(solution)/shard_map/ppermute | solution.py:67
  152.4 0.8 convolution_convert_fusion.1
  153.1 6.2 %collective-permute-done.3 = bf16[512,1,64]{0,2,1:T(8,128)(2,1)S(1)} collective-permute-done((bf16[512,1,64]{0,2,1:T(8,128)(2,1)S(1)}, bf16[512,1,64]{0,2,1:T(8,128)(2,1)S(1)}, u32[]{:S(2)}, u32[]{:S(2)}) %collective-permute-start.3) | collective-permute-done | bytes 65568 | tf_op jit(solution)/shard_map/ppermute | solution.py:67
  159.3 0.8 convolution_convert_fusion.2
  160.1 6.4 %collective-permute-done.4 = bf16[512,1,64]{0,2,1:T(8,128)(2,1)S(1)} collective-permute-done((bf16[512,1,64]{0,2,1:T(8,128)(2,1)S(1)}, bf16[512,1,64]{0,2,1:T(8,128)(2,1)S(1)}, u32[]{:S(2)}, u32[]{:S(2)}) %collective-permute-start.4) | collective-permute-done | bytes 65568 | tf_op jit(solution)/shard_map/ppermute | solution.py:67
  166.5 31.6 %all-gather = bf16[4096,64]{0,1:T(8,128)(2,1)S(1)} all-gather(bf16[512,64]{0,1:T(8,128)(2,1)S(1)} %convolution_convert_fusion.2), channel_id=2, replica_groups=mesh['ep'=8,'tp'=4] {'ep'}, dimensions={0}, use_global_device_ids=true | all-gather | bytes 589824 | tf_op jit(solution)/shard_map/all_gather | solution.py:79
  198.5 2.1 collective-permute-start.6
  200.6 0.7 dynamic-slice_bitcast_fusion.1
  201.3 4.4 %collective-permute-done.6 = bf16[512,1,64]{0,2,1:T(8,128)(2,1)S(1)} collective-permute-done((bf16[512,1,64]{0,2,1:T(8,128)(2,1)S(1)}, bf16[512,1,64]{0,2,1:T(8,128)(2,1)S(1)}, u32[]{:S(2)}, u32[]{:S(2)}) %collective-permute-start.6) | collective-permute-done | bytes 65568 | tf_op jit(solution)/shard_map/ppermute | solution.py:67
  206.1 16.9 %while.15 = (s32[]{:T(128)}, f32[1,4,512]{2,1,0:T(4,128)S(1)}, f32[1,4,512]{2,1,0:T(4,128)S(1)}, f32[1,4,512,64]{2,3,1,0:T(8,128)S(1)}, s32[8]{0:T(128)S(1)}, /*...) while((s32[]{:T(128)}, f32[1,4,512]{2,1,0:T(4,128)S(1)}, ...), condition=%wide.region_6.7_spmd.clone, body=%wide.region_1.6_spmd.clone.sunk | while | flops 288889856 | bytes 15282553 | solution.py:116
  206.1 0.7 dynamic_slice.85
  207.5 5.6 %conditional.3 = ((f32[1,4,512]{2,1,0:T(4,128)S(1)}, f32[1,4,512]{2,1,0:T(4,128)S(1)}, f32[1,4,512,64]{2,3,1,0:T(8,128)S(1)})) conditional(s32[]{:T(128)} %convert_element_type.125, (f32[1,4,512]{2,1,0:T(4,128)S(1)}, f32[1,4,512]{2,1,0:T(4,128)S(1)}, f32[1,4,512,64]{2,3,1,0:T(8,128)S(1)}) %tuple.48, (s32[]{:T(128)}, s32[]{:T(128)}, ...), branch_computations={%region_2.2_spmd, %region_3.5_spmd} | conditional | flops 288889856 | bytes 15280214 | solution.py:114
  207.5 0.8 dynamic-slice_bitcast_fusion
  208.6 1.2 fusion.6
  209.8 1.7 fusion.14
  211.5 1.5 fusion.5
  213.1 0.7 dynamic_slice.85
  214.5 0.7 dynamic_slice.85
  215.9 0.7 dynamic_slice.85
  217.4 0.7 dynamic_slice.85
  218.8 0.7 dynamic_slice.85
  220.2 0.7 dynamic_slice.85
  221.6 0.7 dynamic_slice.85
  223.2 0.7 copy.38
  223.9 3.4 %all-to-all-start = ((bf16[4,128,256]{1,2,0:T(8,128)(2,1)}), bf16[4,128,256]{1,2,0:T(8,128)(2,1)S(1)}, u32[]{:S(2)}, u32[]{:S(2)}) async-start(bf16[4,128,256]{1,2,0:T(8,128)(2,1)} %copy.38), calls=%async_computation | async-start | bytes 524288 | tf_op jit(solution)/shard_map/all_to_all | solution.py:125
  227.4 2.8 copy.45
  230.1 3.2 %all-to-all-done = bf16[4,128,256]{1,2,0:T(8,128)(2,1)S(1)} async-done(((bf16[4,128,256]{1,2,0:T(8,128)(2,1)}), bf16[4,128,256]{1,2,0:T(8,128)(2,1)S(1)}, u32[]{:S(2)}, u32[]{:S(2)}) %all-to-all-start) | async-done | bytes 262176 | tf_op jit(solution)/shard_map/all_to_all | solution.py:125
  233.3 42.0 %all-to-all-start.2 = ((bf16[32,8,2048]{2,0,1:T(8,128)(2,1)}), bf16[32,8,2048]{2,0,1:T(8,128)(2,1)S(1)}, u32[]{:S(2)}, u32[]{:S(2)}) async-start(bf16[32,8,2048]{2,0,1:T(8,128)(2,1)} %copy.45), calls=%async_computation.3 | async-start | bytes 2097152 | tf_op jit(solution)/shard_map/all_to_all | solution.py:183
  275.5 3.0 multiply_reduce_fusion.1
  278.5 1.0 multiply_convert_fusion.1
  279.5 21.4 %all-to-all-done.2 = bf16[32,8,2048]{2,0,1:T(8,128)(2,1)S(1)} async-done(((bf16[32,8,2048]{2,0,1:T(8,128)(2,1)}), bf16[32,8,2048]{2,0,1:T(8,128)(2,1)S(1)}, u32[]{:S(2)}, u32[]{:S(2)}) %all-to-all-start.2) | async-done | bytes 1048608 | tf_op jit(solution)/shard_map/all_to_all | solution.py:183
  301.5 0.9 gather_fusion.1
  303.0 1.5 multiply_reduce_fusion
  304.7 0.8 multiply_convert_fusion.2
  (112 shorter events, 6.4 us)
Async XLA Ops:
  7.2 145.2 %copy-start = (bf16[2048,256]{1,0:T(8,128)(2,1)S(1)}, bf16[2048,256]{1,0:T(8,128)(2,1)}, u32[]{:S(2)}) copy-start(bf16[2048,256]{1,0:T(8,128)(2,1)} %param.23) | copy-start | bytes 3145732
  7.2 31.8 %copy-start.2 = (bf16[256,2048]{1,0:T(8,128)(2,1)S(1)}, bf16[256,2048]{1,0:T(8,128)(2,1)}, u32[]{:S(2)}) copy-start(bf16[256,2048]{1,0:T(8,128)(2,1)} %param.28) | copy-start | bytes 3145732
  7.2 32.1 %copy-start.5 = (f32[2048]{0:T(1024)S(1)}, f32[2048]{0:T(1024)}, u32[]{:S(2)}) copy-start(f32[2048]{0:T(1024)} %param.31) | copy-start | bytes 24580
  7.2 102.5 %all-gather.4.cloned.1.call-start = ((), (), s32[]{:S(2)}) async-start(), calls=%async_computation.5 | async-start | bytes 5242880 | tf_op jit(solution)/shard_map/all_gather | solution.py:162
  76.1 151.3 %reduce-scatter.2.cloned.1.call-start = ((), (), s32[]{:S(2)}) async-start(), calls=%async_computation.4 | async-start | bytes 5242880 | tf_op jit(solution)/shard_map/reduce_scatter | solution.py:174
  109.7 7.5 %copy-start.10 = (bf16[128,8,2048]{2,1,0:T(8,128)(2,1)S(1)}, bf16[128,8,2048]{2,1,0:T(8,128)(2,1)}, u32[]{:S(2)}) copy-start(bf16[128,8,2048]{2,1,0:T(8,128)(2,1)} %all-gather.4.cloned.1.call-done) | copy-start | bytes 12582916
  109.7 7.5 %copy-start.11 = (bf16[1,2048,896]{2,1,0:T(8,128)(2,1)S(1)}, bf16[1,2048,896]{2,1,0:T(8,128)(2,1)}, u32[]{:S(2)}) copy-start(bf16[1,2048,896]{2,1,0:T(8,128)(2,1)} %param.32) | copy-start | bytes 11010052
  117.2 4.8 %copy-start.12 = (bf16[1,896,2048]{2,1,0:T(8,128)(2,1)S(1)}, bf16[1,896,2048]{2,1,0:T(8,128)(2,1)}, u32[]{:S(2)}) copy-start(bf16[1,896,2048]{2,1,0:T(8,128)(2,1)} %param.34) | copy-start | bytes 11010052
  128.0 1.6 copy-start.1
  128.0 2.1 copy-start.6
  129.6 1.1 copy-start.3
  130.1 29.2 %copy-start.4 = (bf16[2048,64]{0,1:T(8,128)(2,1)S(1)}, bf16[2048,64]{0,1:T(8,128)(2,1)}, u32[]{:S(2)}) copy-start(bf16[2048,64]{0,1:T(8,128)(2,1)} %param.25) | copy-start | bytes 786436
  131.4 7.0 %collective-permute-start = (bf16[512,1,64]{0,2,1:T(8,128)(2,1)S(1)}, bf16[512,1,64]{0,2,1:T(8,128)(2,1)S(1)}, u32[]{:S(2)}, u32[]{:S(2)}) collective-permute-start(bf16[512,1,64]{0,2,1:T(8,128)(2,1)S(1)} %fusion.46), channel_id=1, source_target_pairs={{0,4},{4,8},{8,12},{12,16},{16,20},{20,24},{24,28},{28,0},{1,5},{5... | collective-permute-start | bytes 196616 | tf_op jit(solution)/shard_map/ppermute | solution.py:67
  138.4 7.0 %collective-permute-start.1 = (bf16[512,1,64]{0,2,1:T(8,128)(2,1)S(1)}, bf16[512,1,64]{0,2,1:T(8,128)(2,1)S(1)}, u32[]{:S(2)}, u32[]{:S(2)}) collective-permute-start(bf16[512,1,64]{0,2,1:T(8,128)(2,1)S(1)} %collective-permute-done), channel_id=1, source_target_pairs={{0,4},{4,8},{8,12},{12,16},{16,20},{20,24},{24,28},{28,0},{1,5},{5... | collective-permute-start | bytes 196616 | tf_op jit(solution)/shard_map/ppermute | solution.py:67
  145.4 7.0 %collective-permute-start.2 = (bf16[512,1,64]{0,2,1:T(8,128)(2,1)S(1)}, bf16[512,1,64]{0,2,1:T(8,128)(2,1)S(1)}, u32[]{:S(2)}, u32[]{:S(2)}) collective-permute-start(bf16[512,1,64]{0,2,1:T(8,128)(2,1)S(1)} %collective-permute-done.1), channel_id=1, source_target_pairs={{0,4},{4,8},{8,12},{12,16},{16,20},{20,24},{24,28},{28,0},{1,5},{5... | collective-permute-start | bytes 196616 | tf_op jit(solution)/shard_map/ppermute | solution.py:67
  152.4 7.0 %collective-permute-start.3 = (bf16[512,1,64]{0,2,1:T(8,128)(2,1)S(1)}, bf16[512,1,64]{0,2,1:T(8,128)(2,1)S(1)}, u32[]{:S(2)}, u32[]{:S(2)}) collective-permute-start(bf16[512,1,64]{0,2,1:T(8,128)(2,1)S(1)} %collective-permute-done.2), channel_id=1, source_target_pairs={{0,4},{4,8},{8,12},{12,16},{16,20},{20,24},{24,28},{28,0},{1,5},{5... | collective-permute-start | bytes 196616 | tf_op jit(solution)/shard_map/ppermute | solution.py:67
  159.3 7.2 %collective-permute-start.4 = (bf16[512,1,64]{0,2,1:T(8,128)(2,1)S(1)}, bf16[512,1,64]{0,2,1:T(8,128)(2,1)S(1)}, u32[]{:S(2)}, u32[]{:S(2)}) collective-permute-start(bf16[512,1,64]{0,2,1:T(8,128)(2,1)S(1)} %collective-permute-done.3), channel_id=1, source_target_pairs={{0,4},{4,8},{8,12},{12,16},{16,20},{20,24},{24,28},{28,0},{1,5},{5... | collective-permute-start | bytes 196616 | tf_op jit(solution)/shard_map/ppermute | solution.py:67
  166.5 32.0 %collective-permute-start.5 = (bf16[512,1,64]{0,2,1:T(8,128)(2,1)S(1)}, bf16[512,1,64]{0,2,1:T(8,128)(2,1)S(1)}, u32[]{:S(2)}, u32[]{:S(2)}) collective-permute-start(bf16[512,1,64]{0,2,1:T(8,128)(2,1)S(1)} %collective-permute-done.4), channel_id=1, source_target_pairs={{0,4},{4,8},{8,12},{12,16},{16,20},{20,24},{24,28},{28,0},{1,5},{5... | collective-permute-start | bytes 196616 | tf_op jit(solution)/shard_map/ppermute | solution.py:67
  198.5 7.2 %collective-permute-start.6 = (bf16[512,1,64]{0,2,1:T(8,128)(2,1)S(1)}, bf16[512,1,64]{0,2,1:T(8,128)(2,1)S(1)}, u32[]{:S(2)}, u32[]{:S(2)}) collective-permute-start(bf16[512,1,64]{0,2,1:T(8,128)(2,1)S(1)} %collective-permute-done.5), channel_id=1, source_target_pairs={{0,4},{4,8},{8,12},{12,16},{16,20},{20,24},{24,28},{28,0},{1,5},{5... | collective-permute-start | bytes 196616 | tf_op jit(solution)/shard_map/ppermute | solution.py:67
  223.0 52.2 %copy-start.9 = (f32[256,2]{0,1:T(2,128)S(1)}, f32[256,2]{0,1:T(2,128)}, u32[]{:S(2)}) copy-start(f32[256,2]{0,1:T(2,128)} %param.30) | copy-start | bytes 6148
  223.9 9.4 %all-to-all-start = ((bf16[4,128,256]{1,2,0:T(8,128)(2,1)}), bf16[4,128,256]{1,2,0:T(8,128)(2,1)S(1)}, u32[]{:S(2)}, u32[]{:S(2)}) async-start(bf16[4,128,256]{1,2,0:T(8,128)(2,1)} %copy.38), calls=%async_computation | async-start | bytes 524288 | tf_op jit(solution)/shard_map/all_to_all | solution.py:125
  230.1 48.4 %copy-start.7 = (f32[2048]{0:T(1024)S(1)}, f32[2048]{0:T(1024)}, u32[]{:S(2)}) copy-start(f32[2048]{0:T(1024)} %param.27) | copy-start | bytes 24580
  233.3 67.6 %all-to-all-start.2 = ((bf16[32,8,2048]{2,0,1:T(8,128)(2,1)}), bf16[32,8,2048]{2,0,1:T(8,128)(2,1)S(1)}, u32[]{:S(2)}, u32[]{:S(2)}) async-start(bf16[32,8,2048]{2,0,1:T(8,128)(2,1)} %copy.45), calls=%async_computation.3 | async-start | bytes 2097152 | tf_op jit(solution)/shard_map/all_to_all | solution.py:183
  301.4 3.3 %copy-start.8 = (f32[2048]{0:T(1024)S(1)}, f32[2048]{0:T(1024)}, u32[]{:S(2)}) copy-start(f32[2048]{0:T(1024)} %param.35) | copy-start | bytes 24580
Sparse Core Ops, SparseCore 0:
  76.2 33.4 all-gather.3
  128.1 44.5 reduce-scatter.1
